TPU v7x, 32 devices: a whole 2x2x4 slice. The times are simulated.
32 devices in a mesh: ep: 8 (over z, y), tp: 4 (over x, core).
Axes of the slice: x: 2, y: 2, z: 4, core: 2. Of those that a mesh axis runs over, the one named last changes fastest.
Arguments:
- query_rows: bfloat16 [8192, 1024], P('ep', 'tp'), may hold values from -140 to 140
- key_rows: bfloat16 [8192, 256], P('ep', 'tp'), may hold values from -4.5 to 4.5
- value_rows: bfloat16 [8192, 256], P('ep', 'tp'), may hold values from -6 to 6
- sink_logit: float32 [16], P('tp'), may hold values from 1 to 6
- out_weight: bfloat16 [1024, 2048], P('tp'), may hold values from -0.1875 to 0.1875
- routed_rows: bfloat16 [4096, 2048], P(('ep', 'tp')), may hold values from -6 to 6
- norm_gain: float32 [2048], replicated, may hold values from 0.1 to 1.9
- routing: int32 [4096, 2], P(('ep', 'tp')), may hold values from 0 to 7, all different within a row; in each aligned block of 128 rows (0 to 127, 128 to 255, ...) at most 36 rows name the same one
- route_weight: float32 [4096, 2], P(('ep', 'tp')), may hold values from 0.2 to 1
- gate_weight: bfloat16 [8, 2048, 7168], P('ep', None, 'tp'), may hold values from -0.125 to 0.125
- up_weight: bfloat16 [8, 2048, 7168], P('ep', None, 'tp'), may hold values from -0.125 to 0.125
- down_weight: bfloat16 [8, 7168, 2048], P('ep', 'tp'), may hold values from -0.0625 to 0.0625
Outputs:
- mixed_rows: bfloat16 [8192, 2048], P(('ep', 'tp'))
- expert_mix: bfloat16 [4096, 2048], P(('ep', 'tp'))
Inputs may be any that keep to these rules, and one draw needn't show every extreme that they name: `routing`: each token names 2 different experts. Within the 128 rows of one device no expert is named by more than 36 rows, and in every draw some device's rows name some expert exactly 36 times.
All inputs are finite; a program needn't handle non-finite values.
Results may differ from a plain program's by a relative error of at most 0.012.
Values may be sent and summed in bfloat16 or wider, within the bound.
A program may use at most 128 MiB of HBM per device.

v0:
```python
import jax
import jax.numpy as jnp
from jax import lax
from jax.sharding import PartitionSpec as P

HEAD_DIM = 64
WINDOW = 128
EPS = 1e-06


def padded_2(value, sides, width):
    for axis, dim in sides:
        peers, length = (lax.axis_size(axis), value.shape[dim])
        up = [(i, (i + 1) % peers) for i in range(peers - 1)]
        down = [(j, i) for i, j in up]
        last = lax.slice_in_dim(value, length - width, length, axis=dim)
        leading = lax.slice_in_dim(value, 0, width, axis=dim)
        before = lax.ppermute(last, axis, up)
        after = lax.ppermute(leading, axis, down)
        value = jnp.concatenate([before, value, after], axis=dim)
    return value


def expert_hidden(arrived, gate_weight, up_weight):
    gate_pre = jnp.einsum(
        "scd,df->scf", arrived, gate_weight[0], preferred_element_type=jnp.float32
    )
    up_pre = jnp.einsum("scd,df->scf", arrived, up_weight[0], preferred_element_type=jnp.float32)
    return (jax.nn.silu(gate_pre) * up_pre).astype(jnp.bfloat16)


def window_attention(query_rows, key_rows, value_rows, sink_logit):
    row_count = query_rows.shape[0]
    kv_here = key_rows.shape[1] // HEAD_DIM
    group_size = query_rows.shape[1] // (kv_here * HEAD_DIM)
    block_rows = min(512, row_count)
    joined = jnp.concatenate([key_rows, value_rows], axis=1)
    padded = padded_2(joined, (("ep", 0),), WINDOW)
    seq_total = row_count * lax.axis_size("ep")
    offset = lax.axis_index("ep") * row_count
    sink_col = sink_logit.reshape(kv_here, group_size)[:, :, None]
    score_scale = HEAD_DIM ** (-0.5)

    def one_block(block_index):
        first_row = block_index * block_rows
        query_block = lax.dynamic_slice_in_dim(query_rows, first_row, block_rows, 0).reshape(
            block_rows, kv_here, group_size, HEAD_DIM
        )
        key_span = lax.dynamic_slice_in_dim(padded, first_row, block_rows + 2 * WINDOW, 0)
        key_block = key_span[:, : kv_here * HEAD_DIM].reshape(-1, kv_here, HEAD_DIM)
        value_block = key_span[:, kv_here * HEAD_DIM :].reshape(-1, kv_here, HEAD_DIM)
        scores = (
            jnp.einsum("qkgd,skd->kgqs", query_block, key_block, preferred_element_type=jnp.float32)
            * score_scale
        )
        query_pos = first_row + jnp.arange(block_rows, dtype=jnp.int32)
        key_pos = first_row - WINDOW + jnp.arange(block_rows + 2 * WINDOW, dtype=jnp.int32)
        global_pos = offset + key_pos
        inside = (
            (jnp.abs(key_pos[None, :] - query_pos[:, None]) <= WINDOW)
            & (global_pos >= 0)[None, :]
            & (global_pos < seq_total)[None, :]
        )
        scores = jnp.where(inside, scores, -jnp.inf)
        row_peak = jnp.maximum(jnp.max(scores, axis=-1), sink_col)
        weights = jnp.exp(scores - row_peak[..., None])
        total_weight = jnp.sum(weights, axis=-1) + jnp.exp(sink_col - row_peak)
        attended = jnp.einsum(
            "kgqs,skd->qkgd",
            weights.astype(jnp.bfloat16),
            value_block,
            preferred_element_type=jnp.float32,
        )
        attended = attended / jnp.transpose(total_weight, (2, 0, 1))[..., None]
        return attended.reshape(block_rows, -1).astype(jnp.bfloat16)

    pieces = lax.map(one_block, jnp.arange(row_count // block_rows, dtype=jnp.int32))
    return pieces.reshape(row_count, -1)


def body(
    query_rows,
    key_rows,
    value_rows,
    sink_logit,
    out_weight,
    routed_rows,
    norm_gain,
    routing,
    route_weight,
    gate_weight,
    up_weight,
    down_weight,
):
    attended = window_attention(query_rows, key_rows, value_rows, sink_logit)
    projected = lax.psum_scatter(
        jnp.dot(attended, out_weight, preferred_element_type=jnp.float32).astype(jnp.bfloat16),
        "tp",
        scatter_dimension=0,
        tiled=True,
    )
    token_count, model_width = routed_rows.shape
    top_count = routing.shape[1]
    experts = lax.axis_size("ep")
    capacity = token_count * top_count * 9 // (8 * experts)
    values = routed_rows.astype(jnp.float32)
    normed = (
        values * lax.rsqrt(jnp.mean(values * values, axis=-1, keepdims=True) + EPS) * norm_gain
    ).astype(jnp.bfloat16)
    chosen = routing.reshape(-1)
    onehot = (chosen[:, None] == jnp.arange(experts, dtype=jnp.int32)[None, :]).astype(jnp.int32)
    before = jnp.cumsum(onehot, axis=0) - onehot
    slot_index = jnp.sum(before * onehot, axis=1)
    target = chosen * capacity + slot_index
    outgoing = (
        jnp.zeros((experts * capacity, model_width), jnp.bfloat16)
        .at[target]
        .set(jnp.repeat(normed, top_count, axis=0))
    )
    outgoing = outgoing.reshape(experts, capacity, model_width)
    hidden = expert_hidden(
        lax.all_gather(
            lax.all_to_all(outgoing, "ep", split_axis=0, concat_axis=0, tiled=True),
            "tp",
            axis=0,
            tiled=True,
        ),
        gate_weight,
        up_weight,
    )
    rounded = jnp.einsum(
        "scf,fd->scd", hidden, down_weight[0], preferred_element_type=jnp.float32
    ).astype(jnp.bfloat16)
    summed = lax.psum_scatter(
        lax.optimization_barrier(rounded).astype(jnp.float32).astype(jnp.bfloat16),
        "tp",
        scatter_dimension=0,
        tiled=True,
    ).astype(jnp.float32)
    results = lax.all_to_all(
        summed.astype(jnp.bfloat16), "ep", split_axis=0, concat_axis=0, tiled=True
    ).astype(summed.dtype)
    slot_results = results.reshape(experts * capacity, model_width)
    picked = slot_results[target] * route_weight.reshape(-1)[:, None]
    expert_mix = jnp.sum(picked.reshape(token_count, top_count, model_width), axis=1).astype(
        jnp.bfloat16
    )
    return (projected, expert_mix)


def solution(mesh):
    in_specs = (
        P("ep", "tp"),
        P("ep", "tp"),
        P("ep", "tp"),
        P("tp"),
        P("tp", None),
        P(("ep", "tp"), None),
        P(),
        P(("ep", "tp"), None),
        P(("ep", "tp"), None),
        P("ep", None, "tp"),
        P("ep", None, "tp"),
        P("ep", "tp", None),
    )
    out_specs = (P(("ep", "tp"), None), P(("ep", "tp"), None))
    return jax.shard_map(body, mesh=mesh, in_specs=in_specs, out_specs=out_specs, check_vma=False)
```

profile of v0, /device:TPU:0, one launch (start us, length us, event | category | flops | bytes accessed | tf_op | source)
XLA Modules:
  0.0 254.0 jit_solution(6978425806556693117)
XLA Ops:
  7.2 0.9 copy.28
  8.1 0.1 eq.29
  8.2 0.1 eq.25
  8.4 0.7 broadcast_multiply_fusion
  9.1 0.6 reduce-window.6
  9.6 0.2 slice_reduce_fusion
  10.0 0.1 mul.81
  10.1 1.2 fusion.47
  11.4 1.2 fusion.49
  12.6 0.6 broadcast_in_dim.38
  13.3 1.2 reshape.293
  14.6 3.1 %scatter_custom_fusion = bf16[288,2048]{1,0:T(8,128)(2,1)S(1)} fusion(s32[256]{0:T(256)S(1)} %bitcast.135, bf16[256,2048]{1,0:T(8,128)(2,1)} %reshape.293, bf16[]{:T(256)} %constant.85.clone.1), kind=kCustom, calls=%fused_computation.52 | custom fusion | bytes 1180160 | tf_op jit(solution)/shard_map/scatter | solution.py:118
  17.7 0.3 reshape.276
  18.0 38.5 %all_to_all.10 = bf16[8,36,2048]{2,1,0:T(8,128)(2,1)S(1)} all-to-all(bf16[8,36,2048]{2,1,0:T(8,128)(2,1)S(1)} %reshape.276), channel_id=1, replica_groups=mesh['ep'=8,'tp'=4] {'ep'}, dimensions={0} | all-to-all | bytes 2359296 | tf_op jit(solution)/shard_map/all_to_all | solution.py:123
  56.5 1.7 copy.30
  58.2 36.5 %all-gather.2.cloned.1.call-done = bf16[32,36,2048]{2,0,1:T(8,128)(2,1)} async-done(((bf16[8,36,2048]{2,0,1:T(8,128)(2,1)}), bf16[32,36,2048]{2,0,1:T(8,128)(2,1)}) %all-gather.2.cloned.1.call-update) | async-done | bytes 4718608 | tf_op jit(solution)/shard_map/all_gather | solution.py:122
  94.8 19.5 %fusion.28 = f32[32,36,1792]{2,1,0:T(8,128)} fusion(bf16[1,2048,1792]{2,1,0:T(8,128)(2,1)} %param.24, bf16[32,36,2048]{2,0,1:T(8,128)(2,1)} %all-gather.2.cloned.1.call-done), kind=kOutput, calls=%fused_computation.37 | convolution fusion | flops 8455716864 | bytes 20316160 | tf_op jit(solution)/shard_map/scd,df->scf/dot_general | solution.py:28
  114.3 33.8 %fusion.40 = bf16[32,36,2048]{2,1,0:T(8,128)(2,1)} fusion(bf16[1,1792,2048]{2,1,0:T(8,128)(2,1)} %param.25, f32[32,36,1792]{2,1,0:T(8,128)} %fusion.28, bf16[1,2048,1792]{2,1,0:T(8,128)(2,1)} %param.23, bf16[32,36,2048]{2,0,1:T(8,128)(2,1)} %all-gather.2.cloned.1.call-done), kind=kOutput, calls=%fused_computation.44 | convolution fusion | flops 16926179328 | bytes 32374784 | tf_op jit(solution)/shard_map/scf,fd->scd/dot_general | solution.py:131
  148.2 3.5 %collective-permute-start = (bf16[128,128]{0,1:T(8,128)(2,1)S(1)}, bf16[128,128]{0,1:T(8,128)(2,1)S(1)}, u32[]{:S(2)}, u32[]{:S(2)}) collective-permute-start(bf16[128,128]{0,1:T(8,128)(2,1)S(1)} %get-tuple-element.131), channel_id=1, source_target_pairs={{0,4},{4,8},{8,12},{12,16},{16,20},{20,24},{24,28},{1,5},{5,9},{9,... | collective-permute-start | bytes 98312 | tf_op jit(solution)/shard_map/ppermute | solution.py:18
  151.8 1.3 collective-permute-start.1
  153.1 0.3 collective-permute-done
  153.3 4.2 %collective-permute-done.1 = bf16[128,128]{0,1:T(8,128)(2,1)S(1)} collective-permute-done((bf16[128,128]{0,1:T(8,128)(2,1)S(1)}, bf16[128,128]{0,1:T(8,128)(2,1)S(1)}, u32[]{:S(2)}, u32[]{:S(2)}) %collective-permute-start.1) | collective-permute-done | bytes 32800 | tf_op jit(solution)/shard_map/ppermute | solution.py:19
  157.6 25.5 %while.12 = (s32[]{:T(128)}, bf16[2,512,256]{2,1,0:T(8,128)(2,1)S(1)}, s32[2]{0:T(128)S(1)}, bf16[1280,128]{0,1:T(8,128)(2,1)S(1)}, s32[]{:T(128)}, /*index=5*/b...) while((s32[]{:T(128)}, ...), condition=%wide.region_3.4_spmd, body=%wide.region_0.3_spmd.sunk | while | flops 422191360 | bytes 48526672 | solution.py:77
  157.9 0.7 dynamic_slice.23
  159.2 0.8 fusion.69
  160.1 0.1 copy.47
  160.2 1.2 fusion.70
  161.5 2.6 %copy-done.1 = f32[768,512,4]{1,0,2:T(8,128)} copy-done((f32[768,512,4]{1,0,2:T(8,128)}, f32[768,512,4]{1,0,2:T(8,128)S(1)}, u32[]{:S(2)}) %copy-start.1) | copy-done | bytes 6291480 | tf_op jit(solution)/shard_map/while
  164.1 1.4 fusion.71
  165.5 5.0 %fusion.73 = bf16[512,1,4,64]{0,3,2,1:T(8,128)(2,1)S(1)} fusion(f32[768,512,4]{1,0,2:T(8,128)} %copy-done.1, f32[4,512]{1,0:T(4,128)S(1)} %broadcast_maximum_fusion.2, pred[512,768]{0,1:T(8,128)(4,1)S(1)} %fusion.69, f32[512,4]{0,1:T(4,128)S(1)} %fusion.72, bf16[1280,128]{0,1:T(8,128)(2,1)S(1)} %get-tuple-element.215, s32[]{:T(128)S(6)} %select_n.57, ...), kind=kOutput, calls=%fused_computation.15.clone.1 | convolution fusion | flops 207880192 | bytes 7061512 | tf_op jit(solution)/shard_map/while/body/eval_jaxpr/kgqs,skd->qkgd/dot_general | solution.py:68
  170.5 0.1 copy.48
  170.7 0.7 dynamic_slice.23
  172.1 0.8 fusion.69
  172.9 0.1 copy.47
  173.1 1.2 fusion.70
  174.4 2.6 %copy-done.1 = f32[768,512,4]{1,0,2:T(8,128)} copy-done((f32[768,512,4]{1,0,2:T(8,128)}, f32[768,512,4]{1,0,2:T(8,128)S(1)}, u32[]{:S(2)}) %copy-start.1) | copy-done | bytes 6291480 | tf_op jit(solution)/shard_map/while
  176.9 1.4 fusion.71
  178.4 4.6 %fusion.73 = bf16[512,1,4,64]{0,3,2,1:T(8,128)(2,1)S(1)} fusion(f32[768,512,4]{1,0,2:T(8,128)} %copy-done.1, f32[4,512]{1,0:T(4,128)S(1)} %broadcast_maximum_fusion.2, pred[512,768]{0,1:T(8,128)(4,1)S(1)} %fusion.69, f32[512,4]{0,1:T(4,128)S(1)} %fusion.72, bf16[1280,128]{0,1:T(8,128)(2,1)S(1)} %get-tuple-element.215, s32[]{:T(128)S(6)} %select_n.57, ...), kind=kOutput, calls=%fused_computation.15.clone.1 | convolution fusion | flops 207880192 | bytes 7061512 | tf_op jit(solution)/shard_map/while/body/eval_jaxpr/kgqs,skd->qkgd/dot_general | solution.py:68
  182.9 0.1 copy.48
  183.2 3.2 %convolution_convert_fusion = bf16[1024,2048]{1,0:T(8,128)(2,1)} fusion(bf16[1024,256]{1,0:T(8,128)(2,1)S(1)} %bitcast.131, bf16[256,2048]{1,0:T(8,128)(2,1)S(1)} %copy-done), kind=kOutput, calls=%fused_computation.45 | convolution fusion | flops 1075838976 | bytes 5767168 | tf_op jit(solution)/shard_map/dot_general | solution.py:97
  186.4 13.3 %reduce-scatter.5.cloned.1.call-done = bf16[8,36,2048]{2,1,0:T(8,128)(2,1)} async-done(((bf16[32,36,2048]{2,1,0:T(8,128)(2,1)}), bf16[8,36,2048]{2,1,0:T(8,128)(2,1)}) %reduce-scatter.5.cloned.1.call-update) | async-done | bytes 1179664 | tf_op jit(solution)/shard_map/reduce_scatter | solution.py:134
  199.6 5.5 %all-to-all-start.1 = ((bf16[8,36,2048]{2,1,0:T(8,128)(2,1)}), bf16[8,36,2048]{2,1,0:T(8,128)(2,1)}, u32[]{:S(2)}, u32[]{:S(2)}) async-start(bf16[8,36,2048]{2,1,0:T(8,128)(2,1)} %reduce-scatter.5.cloned.1.call-done), calls=%async_computation.3 | async-start | bytes 2621440 | tf_op jit(solution)/shard_map/all_to_all | solution.py:140
  205.3 31.2 %all-to-all-done.1 = bf16[8,36,2048]{2,1,0:T(8,128)(2,1)} async-done(((bf16[8,36,2048]{2,1,0:T(8,128)(2,1)}), bf16[8,36,2048]{2,1,0:T(8,128)(2,1)}, u32[]{:S(2)}, u32[]{:S(2)}) %all-to-all-start.1) | async-done | bytes 1179680 | tf_op jit(solution)/shard_map/all_to_all | solution.py:140
  236.5 1.4 reshape.280
  237.9 2.7 %gather_fusion = f32[256,2048]{1,0:T(8,128)} fusion(f32[288,2048]{1,0:T(8,128)S(1)} %reshape.280, s32[1024]{0:T(1024)S(1)} %pad_clamp_fusion), kind=kCustom, calls=%fused_computation | custom fusion | bytes 4195328 | tf_op jit(solution)/shard_map/gather | solution.py:144
  240.6 2.5 gather.6
  243.1 3.9 %multiply_reduce_fusion = bf16[128,2048]{1,0:T(8,128)(2,1)} fusion(f32[128,2,2048]{2,1,0:T(2,128)S(1)} %gather.6, f32[128,2]{1,0:T(8,128)S(1)} %copy.33), kind=kLoop, calls=%fused_computation.46 | loop fusion | flops 786432 | bytes 2622464 | tf_op jit(solution)/shard_map/reduce_sum | solution.py:145
  247.0 0.4 reduce-scatter.3.cloned.1.call-done
  (49 shorter events, 1.1 us)
Async XLA Ops:
  7.2 176.0 %copy-start = (bf16[256,2048]{1,0:T(8,128)(2,1)S(1)}, bf16[256,2048]{1,0:T(8,128)(2,1)}, u32[]{:S(2)}) copy-start(bf16[256,2048]{1,0:T(8,128)(2,1)} %param.18) | copy-start | bytes 3145732
  7.2 87.6 %all-gather.2.cloned.1.call-start = ((), (), s32[]{:S(2)}) async-start(), calls=%async_computation.5 | async-start | bytes 5898240 | tf_op jit(solution)/shard_map/all_gather | solution.py:122
  58.2 141.4 %reduce-scatter.5.cloned.1.call-start = ((), (), s32[]{:S(2)}) async-start(), calls=%async_computation.6 | async-start | bytes 6553600 | tf_op jit(solution)/shard_map/reduce_scatter | solution.py:134
  114.3 33.9 %copy-start.3 = (bf16[1024,64]{0,1:T(8,128)(2,1)S(1)}, bf16[1024,64]{0,1:T(8,128)(2,1)}, u32[]{:S(2)}) copy-start(bf16[1024,64]{0,1:T(8,128)(2,1)} %param.15) | copy-start | bytes 393220
  114.3 33.9 %copy-start.4 = (bf16[1024,64]{0,1:T(8,128)(2,1)S(1)}, bf16[1024,64]{0,1:T(8,128)(2,1)}, u32[]{:S(2)}) copy-start(bf16[1024,64]{0,1:T(8,128)(2,1)} %param.16) | copy-start | bytes 393220
  148.1 9.5 %copy-start.2 = (bf16[1024,256]{1,0:T(8,128)(2,1)S(1)}, bf16[1024,256]{1,0:T(8,128)(2,1)}, u32[]{:S(2)}) copy-start(bf16[1024,256]{1,0:T(8,128)(2,1)} %param.14) | copy-start | bytes 1572868
  148.1 9.5 %copy-start.5 = (f32[4]{0:T(128)S(1)}, f32[4]{0:T(128)}, u32[]{:S(2)}) copy-start(f32[4]{0:T(128)} %param.17) | copy-start | bytes 52
  148.1 99.3 %reduce-scatter.3.cloned.1.call-start = ((), (), s32[]{:S(2)}) async-start(), calls=%async_computation.4 | async-start | bytes 5242880 | tf_op jit(solution)/shard_map/reduce_scatter | solution.py:96
  148.2 5.1 %collective-permute-start = (bf16[128,128]{0,1:T(8,128)(2,1)S(1)}, bf16[128,128]{0,1:T(8,128)(2,1)S(1)}, u32[]{:S(2)}, u32[]{:S(2)}) collective-permute-start(bf16[128,128]{0,1:T(8,128)(2,1)S(1)} %get-tuple-element.131), channel_id=1, source_target_pairs={{0,4},{4,8},{8,12},{12,16},{16,20},{20,24},{24,28},{1,5},{5,9},{9,... | collective-permute-start | bytes 98312 | tf_op jit(solution)/shard_map/ppermute | solution.py:18
  151.8 5.8 %collective-permute-start.1 = (bf16[128,128]{0,1:T(8,128)(2,1)S(1)}, bf16[128,128]{0,1:T(8,128)(2,1)S(1)}, u32[]{:S(2)}, u32[]{:S(2)}) collective-permute-start(bf16[128,128]{0,1:T(8,128)(2,1)S(1)} %get-tuple-element.132), channel_id=1, source_target_pairs={{4,0},{8,4},{12,8},{16,12},{20,16},{24,20},{28,24},{5,1},{9,5},{13... | collective-permute-start | bytes 98312 | tf_op jit(solution)/shard_map/ppermute | solution.py:19
  161.4 2.7 %copy-start.1 = (f32[768,512,4]{1,0,2:T(8,128)}, f32[768,512,4]{1,0,2:T(8,128)S(1)}, u32[]{:S(2)}) copy-start(f32[768,512,4]{1,0,2:T(8,128)S(1)} %get-tuple-element.182) | copy-start | bytes 18874372 | tf_op jit(solution)/shard_map/while
  174.3 2.7 %copy-start.1 = (f32[768,512,4]{1,0,2:T(8,128)}, f32[768,512,4]{1,0,2:T(8,128)S(1)}, u32[]{:S(2)}) copy-start(f32[768,512,4]{1,0,2:T(8,128)S(1)} %get-tuple-element.182) | copy-start | bytes 18874372 | tf_op jit(solution)/shard_map/while
  183.1 22.0 %copy-start.6 = (f32[128,2]{0,1:T(2,128)S(1)}, f32[128,2]{0,1:T(2,128)}, u32[]{:S(2)}) copy-start(f32[128,2]{0,1:T(2,128)} %param.22) | copy-start | bytes 3076
  199.6 36.8 %all-to-all-start.1 = ((bf16[8,36,2048]{2,1,0:T(8,128)(2,1)}), bf16[8,36,2048]{2,1,0:T(8,128)(2,1)}, u32[]{:S(2)}, u32[]{:S(2)}) async-start(bf16[8,36,2048]{2,1,0:T(8,128)(2,1)} %reduce-scatter.5.cloned.1.call-done), calls=%async_computation.3 | async-start | bytes 2621440 | tf_op jit(solution)/shard_map/all_to_all | solution.py:140
Sparse Core Ops, SparseCore 0:
  58.3 36.4 all-gather.1
  148.2 51.3 reduce-scatter.4
  202.7 44.6 reduce-scatter.2
where the time goes:
time: 254 us
  waiting for transfers between devices  86 us (34%)
  matrix products  68.4 us (27%)
  blocking collectives  38.5 us (15%)
  local copies, waits for them, and re-layouts  22.4 us (9%)
  between operations  13.9 us (5%)
  other arithmetic  12.5 us (5%)
  starting transfers between devices  10.4 us (4%)
    all_to_all x1, blocking collectives, body(): lax.all_to_all(outgoing, 'ep', split_axis=0, concat_axis=0, tiled=True)  38.5 us
    all_gather x1, waiting for transfers between devices, body(): lax.all_gather(lax.all_to_all(outgoing, 'ep', split_axis=0, concat_axis=0...  36.5 us
    dot_general x1, matrix products, body(): jnp.einsum('scf,fd->scd', hidden, down_weight[0], preferred_element_type=...  33.8 us
    all_to_all x1, waiting for transfers between devices, body(): lax.all_to_all(summed.astype(jnp.bfloat16), 'ep', split_axis=0, concat_ax...  31.2 us
    dot_general x1, matrix products, expert_hidden(): jnp.einsum('scd,df->scf', arrived, up_weight[0], preferred_element_type=j...  19.5 us
    reduce_scatter x1, waiting for transfers between devices, body(): lax.psum_scatter(lax.optimization_barrier(rounded).astype(jnp.float32).as...  13.3 us
    dot_general x2, matrix products, one_block(): jnp.einsum('kgqs,skd->qkgd', weights.astype(jnp.bfloat16), value_block, p...  9.53 us
    all_to_all x1, starting transfers between devices, body(): lax.all_to_all(summed.astype(jnp.bfloat16), 'ep', split_axis=0, concat_ax...  5.52 us
  transfers between devices with their start and end apart: 6, of which 6 were waited for; matrix products, arithmetic and copies ran while one was open for 13% of the time, Pallas kernels for 0%

commit v1 on v0

--- a/solution.py
+++ b/solution.py
@@ -6,6 +6,19 @@
 HEAD_DIM = 64
 WINDOW = 128
 EPS = 1e-06
+
+
+def gather_around(x, axis, dim):
+    ways = lax.axis_size(axis)
+    up = [(d, (d + 1) % ways) for d in range(ways)]
+    down = [(d, (d - 1) % ways) for d in range(ways)]
+    earlier, later = ([x], [x])
+    for _ in range(ways // 2):
+        earlier.append(lax.ppermute(earlier[-1], axis, up))
+    for _ in range((ways - 1) // 2):
+        later.append(lax.ppermute(later[-1], axis, down))
+    line = jnp.concatenate([*earlier[::-1], *later[1:]], axis=dim)
+    return jnp.roll(line, (lax.axis_index(axis) - ways // 2) * x.shape[dim], axis=dim)
 
 
 def padded_2(value, sides, width):
@@ -119,11 +132,8 @@
     )
     outgoing = outgoing.reshape(experts, capacity, model_width)
     hidden = expert_hidden(
-        lax.all_gather(
-            lax.all_to_all(outgoing, "ep", split_axis=0, concat_axis=0, tiled=True),
-            "tp",
-            axis=0,
-            tiled=True,
+        gather_around(
+            lax.all_to_all(outgoing, "ep", split_axis=0, concat_axis=0, tiled=True), "tp", 0
         ),
         gate_weight,
         up_weight,

time: 254 us -> 259 us (1.020)
  matrix products: 68.4 us -> 58 us
  local copies, waits for them, and re-layouts: 22.4 us -> 32 us
  waiting for transfers between devices: 86 us -> 89.5 us
    ppermute x0 -> x3, waiting for transfers between devices: none -> 40.2 us  [the longest x2 40.2 us: gather_around(): earlier.append(lax.ppermute(earlier[-1], axis, up))]
    all_gather x1 -> x0, waiting for transfers between devices: 36.5 us -> none  [body(): lax.all_gather(lax.all_to_all(outgoing, 'ep', split_axis=0, concat_axis=0...]
    unnamed x15 -> x30, local copies, waits for them, and re-layouts: 1.02 us -> 11.4 us
    dot_general x1, matrix products: 19.5 us -> 12 us  [expert_hidden(): jnp.einsum('scd,df->scf', arrived, gate_weight[0], preferred_element_type...]
    dot_general x1, matrix products: 33.8 us -> 30.8 us  [body(): jnp.einsum('scf,fd->scd', hidden, down_weight[0], preferred_element_type=...]
  transfers between devices with their start and end apart: 6 -> 8, of which waited for: 6 -> 7; matrix products, arithmetic and copies ran while one was open for 13% -> 14% of each run, Pallas kernels for 0% -> 0%
where the time goes in v1:
time: 259 us
  waiting for transfers between devices  89.5 us (35%)
  matrix products  58 us (22%)
  blocking collectives  38.7 us (15%)
  local copies, waits for them, and re-layouts  32 us (12%)
  between operations  14.3 us (6%)
  other arithmetic  12.5 us (5%)
  starting transfers between devices  12.1 us (5%)
    ppermute x2, waiting for transfers between devices, gather_around(): earlier.append(lax.ppermute(earlier[-1], axis, up))  40.2 us
    all_to_all x1, blocking collectives, body(): lax.all_to_all(outgoing, 'ep', split_axis=0, concat_axis=0, tiled=True)  38.7 us
    all_to_all x1, waiting for transfers between devices, body(): lax.all_to_all(summed.astype(jnp.bfloat16), 'ep', split_axis=0, concat_ax...  31.2 us
    dot_general x1, matrix products, body(): jnp.einsum('scf,fd->scd', hidden, down_weight[0], preferred_element_type=...  30.8 us
    reduce_scatter x1, waiting for transfers between devices, body(): lax.psum_scatter(lax.optimization_barrier(rounded).astype(jnp.float32).as...  13.2 us
    dot_general x1, matrix products, expert_hidden(): jnp.einsum('scd,df->scf', arrived, gate_weight[0], preferred_element_type...  12 us
    unnamed x30, local copies, waits for them, and re-layouts  11.4 us
    dot_general x2, matrix products, one_block(): jnp.einsum('kgqs,skd->qkgd', weights.astype(jnp.bfloat16), value_block, p...  9.55 us
  transfers between devices with their start and end apart: 8, of which 7 were waited for; matrix products, arithmetic and copies ran while one was open for 14% of the time, Pallas kernels for 0%

profile of v1, /device:TPU:0, one launch (start us, length us, event | category | flops | bytes accessed | tf_op | source)
XLA Modules:
  0.0 258.9 jit_solution(16411483189059662616)
XLA Ops:
  7.2 0.9 copy.28
  8.4 0.7 broadcast_multiply_fusion
  9.1 0.6 reduce-window.6
  10.1 1.2 fusion.47
  11.4 1.2 fusion.49
  12.6 0.6 broadcast_in_dim.38
  13.3 0.4 reshape.293
  13.8 2.5 scatter_custom_fusion
  16.3 1.2 reshape.276
  17.5 38.7 %all_to_all.10 = bf16[8,36,2048]{2,1,0:T(8,128)(2,1)S(1)} all-to-all(bf16[8,36,2048]{2,1,0:T(8,128)(2,1)} %reshape.276), channel_id=1, replica_groups=mesh['ep'=8,'tp'=4] {'ep'}, dimensions={0} | all-to-all | bytes 2359296 | tf_op jit(solution)/shard_map/all_to_all | solution.py:136
  56.2 0.7 copy.30
  56.9 15.6 %collective-permute-done.2 = bf16[8,36,2048]{2,0,1:T(8,128)(2,1)S(1)} collective-permute-done((bf16[8,36,2048]{2,0,1:T(8,128)(2,1)S(1)}, bf16[8,36,2048]{2,0,1:T(8,128)(2,1)S(1)}, u32[]{:S(2)}, u32[]{:S(2)}) %collective-permute-start.2) | collective-permute-done | bytes 1179680 | tf_op jit(solution)/shard_map/ppermute | solution.py:17
  72.5 1.7 collective-permute-start.4
  74.3 24.6 %collective-permute-done.3 = bf16[8,36,2048]{2,0,1:T(8,128)(2,1)} collective-permute-done((bf16[8,36,2048]{2,0,1:T(8,128)(2,1)S(1)}, bf16[8,36,2048]{2,0,1:T(8,128)(2,1)}, u32[]{:S(2)}, u32[]{:S(2)}) %collective-permute-start.3) | collective-permute-done | bytes 1179680 | tf_op jit(solution)/shard_map/ppermute | solution.py:17
  98.9 1.9 copy_dynamic-update-slice_fusion.4
  100.8 0.7 copy_dynamic-update-slice_fusion.2
  101.6 0.7 copy_dynamic-update-slice_fusion
  102.3 2.3 copy_dynamic-update-slice_fusion.5
  104.6 0.7 copy_dynamic-update-slice_fusion.3
  105.4 0.7 copy_dynamic-update-slice_fusion.1
  106.0 4.0 %copy-done.2 = bf16[64,36,2048]{2,1,0:T(8,128)(2,1)} copy-done((bf16[64,36,2048]{2,1,0:T(8,128)(2,1)}, bf16[64,36,2048]{2,1,0:T(8,128)(2,1)S(1)}, u32[]{:S(2)}) %copy-start.2) | copy-done | bytes 9437208
  110.0 12.0 %fusion.30 = f32[32,36,1792]{2,1,0:T(8,128)} fusion(bf16[1,2048,1792]{2,1,0:T(8,128)(2,1)S(1)} %bitcast.139, bf16[64,36,2048]{2,1,0:T(8,128)(2,1)S(1)} %copy_dynamic-update-slice_fusion.1, s32[]{:T(128)S(6)} %select_n.45), kind=kOutput, calls=%fused_computation.39 | convolution fusion | flops 8455716864 | bytes 20840452 | tf_op jit(solution)/shard_map/scd,df->scf/dot_general | solution.py:38
  122.1 30.8 %fusion.40 = bf16[32,36,2048]{2,1,0:T(8,128)(2,1)} fusion(bf16[1,1792,2048]{2,1,0:T(8,128)(2,1)} %param.25, f32[32,36,1792]{2,1,0:T(8,128)} %fusion.30, bf16[1,2048,1792]{2,1,0:T(8,128)(2,1)} %param.24, bf16[64,36,2048]{2,1,0:T(8,128)(2,1)} %copy-done.2, s32[]{:T(128)S(6)} %select_n.45), kind=kOutput, calls=%fused_computation.44 | convolution fusion | flops 16926179328 | bytes 33816580 | tf_op jit(solution)/shard_map/scf,fd->scd/dot_general | solution.py:141
  153.0 3.5 %collective-permute-start = (bf16[128,128]{0,1:T(8,128)(2,1)S(1)}, bf16[128,128]{0,1:T(8,128)(2,1)S(1)}, u32[]{:S(2)}, u32[]{:S(2)}) collective-permute-start(bf16[128,128]{0,1:T(8,128)(2,1)S(1)} %get-tuple-element.131), channel_id=1, source_target_pairs={{0,4},{4,8},{8,12},{12,16},{16,20},{20,24},{24,28},{1,5},{5,9},{9,... | collective-permute-start | bytes 98312 | tf_op jit(solution)/shard_map/ppermute | solution.py:31
  156.5 1.3 collective-permute-start.1
  158.1 4.2 %collective-permute-done.1 = bf16[128,128]{0,1:T(8,128)(2,1)S(1)} collective-permute-done((bf16[128,128]{0,1:T(8,128)(2,1)S(1)}, bf16[128,128]{0,1:T(8,128)(2,1)S(1)}, u32[]{:S(2)}, u32[]{:S(2)}) %collective-permute-start.1) | collective-permute-done | bytes 32800 | tf_op jit(solution)/shard_map/ppermute | solution.py:32
  162.4 25.6 %while.12 = (s32[]{:T(128)}, bf16[2,512,256]{2,1,0:T(8,128)(2,1)S(1)}, s32[2]{0:T(128)S(1)}, bf16[1280,128]{0,1:T(8,128)(2,1)S(1)}, s32[]{:T(128)}, /*index=5*/b...) while((s32[]{:T(128)}, ...), condition=%wide.region_3.4_spmd, body=%wide.region_0.3_spmd.sunk | while | flops 422191360 | bytes 48526672 | solution.py:90
  162.6 0.7 dynamic_slice.35
  164.0 0.8 fusion.72
  165.0 1.2 fusion.73
  166.3 2.6 copy-done.1
  168.9 1.4 fusion.74
  170.3 5.0 %fusion.76 = bf16[512,1,4,64]{0,3,2,1:T(8,128)(2,1)S(1)} fusion(f32[768,512,4]{1,0,2:T(8,128)} %copy-done.1, f32[4,512]{1,0:T(4,128)S(1)} %broadcast_maximum_fusion.2, pred[512,768]{0,1:T(8,128)(4,1)S(1)} %fusion.72, f32[512,4]{0,1:T(4,128)S(1)} %fusion.75, bf16[1280,128]{0,1:T(8,128)(2,1)S(1)} %get-tuple-element.215, s32[]{:T(128)S(6)} %select_n.72, ...), kind=kOutput, calls=%fused_computation.15.clone.1 | convolution fusion | flops 207880192 | bytes 7061512 | tf_op jit(solution)/shard_map/while/body/eval_jaxpr/kgqs,skd->qkgd/dot_general | solution.py:81
  175.5 0.7 dynamic_slice.35
  176.9 0.8 fusion.72
  177.9 1.2 fusion.73
  179.2 2.6 copy-done.1
  181.7 1.4 fusion.74
  183.2 4.6 %fusion.76 = bf16[512,1,4,64]{0,3,2,1:T(8,128)(2,1)S(1)} fusion(f32[768,512,4]{1,0,2:T(8,128)} %copy-done.1, f32[4,512]{1,0:T(4,128)S(1)} %broadcast_maximum_fusion.2, pred[512,768]{0,1:T(8,128)(4,1)S(1)} %fusion.72, f32[512,4]{0,1:T(4,128)S(1)} %fusion.75, bf16[1280,128]{0,1:T(8,128)(2,1)S(1)} %get-tuple-element.215, s32[]{:T(128)S(6)} %select_n.72, ...), kind=kOutput, calls=%fused_computation.15.clone.1 | convolution fusion | flops 207880192 | bytes 7061512 | tf_op jit(solution)/shard_map/while/body/eval_jaxpr/kgqs,skd->qkgd/dot_general | solution.py:81
  188.0 3.2 %convolution_convert_fusion = bf16[1024,2048]{1,0:T(8,128)(2,1)} fusion(bf16[1024,256]{1,0:T(8,128)(2,1)S(1)} %bitcast.131, bf16[256,2048]{1,0:T(8,128)(2,1)S(1)} %copy-done), kind=kOutput, calls=%fused_computation.45 | convolution fusion | flops 1075838976 | bytes 5767168 | tf_op jit(solution)/shard_map/dot_general | solution.py:110
  191.2 13.2 %reduce-scatter.5.cloned.1.call-done = bf16[8,36,2048]{2,1,0:T(8,128)(2,1)} async-done(((bf16[32,36,2048]{2,1,0:T(8,128)(2,1)}), bf16[8,36,2048]{2,1,0:T(8,128)(2,1)}) %reduce-scatter.5.cloned.1.call-update) | async-done | bytes 1179664 | tf_op jit(solution)/shard_map/reduce_scatter | solution.py:144
  204.4 5.5 %all-to-all-start.1 = ((bf16[8,36,2048]{2,1,0:T(8,128)(2,1)}), bf16[8,36,2048]{2,1,0:T(8,128)(2,1)}, u32[]{:S(2)}, u32[]{:S(2)}) async-start(bf16[8,36,2048]{2,1,0:T(8,128)(2,1)} %reduce-scatter.5.cloned.1.call-done), calls=%async_computation.3 | async-start | bytes 2621440 | tf_op jit(solution)/shard_map/all_to_all | solution.py:150
  210.0 31.2 %all-to-all-done.1 = bf16[8,36,2048]{2,1,0:T(8,128)(2,1)} async-done(((bf16[8,36,2048]{2,1,0:T(8,128)(2,1)}), bf16[8,36,2048]{2,1,0:T(8,128)(2,1)}, u32[]{:S(2)}, u32[]{:S(2)}) %all-to-all-start.1) | async-done | bytes 1179680 | tf_op jit(solution)/shard_map/all_to_all | solution.py:150
  241.2 1.4 reshape.280
  242.6 2.7 %gather_fusion = f32[256,2048]{1,0:T(8,128)} fusion(f32[288,2048]{1,0:T(8,128)S(1)} %reshape.280, s32[1024]{0:T(1024)S(1)} %pad_clamp_fusion), kind=kCustom, calls=%fused_computation | custom fusion | bytes 4195328 | tf_op jit(solution)/shard_map/gather | solution.py:154
  245.3 2.5 gather.6
  247.8 3.9 %multiply_reduce_fusion = bf16[128,2048]{1,0:T(8,128)(2,1)} fusion(f32[128,2,2048]{2,1,0:T(2,128)S(1)} %gather.6, f32[128,2]{1,0:T(8,128)S(1)} %copy.38), kind=kLoop, calls=%fused_computation.46 | loop fusion | flops 786432 | bytes 2622464 | tf_op jit(solution)/shard_map/reduce_sum | solution.py:155
  251.7 0.3 reduce-scatter.3.cloned.1.call-done
  (69 shorter events, 2.7 us)
Async XLA Ops:
  7.2 180.8 %copy-start = (bf16[256,2048]{1,0:T(8,128)(2,1)S(1)}, bf16[256,2048]{1,0:T(8,128)(2,1)}, u32[]{:S(2)}) copy-start(bf16[256,2048]{1,0:T(8,128)(2,1)} %param.18) | copy-start | bytes 3145732
  7.2 197.2 %reduce-scatter.5.cloned.1.call-start = ((), (), s32[]{:S(2)}) async-start(), calls=%async_computation.5 | async-start | bytes 6553600 | tf_op jit(solution)/shard_map/reduce_scatter | solution.py:144
  56.8 15.7 %copy-start.4 = (bf16[8,36,2048]{2,0,1:T(8,128)(2,1)}, bf16[8,36,2048]{2,0,1:T(8,128)(2,1)S(1)}, u32[]{:S(2)}) copy-start(bf16[8,36,2048]{2,0,1:T(8,128)(2,1)S(1)} %copy.30) | copy-start | bytes 3538948
  56.8 15.7 %collective-permute-start.2 = (bf16[8,36,2048]{2,0,1:T(8,128)(2,1)S(1)}, bf16[8,36,2048]{2,0,1:T(8,128)(2,1)S(1)}, u32[]{:S(2)}, u32[]{:S(2)}) collective-permute-start(bf16[8,36,2048]{2,0,1:T(8,128)(2,1)S(1)} %copy.30), channel_id=1, source_target_pairs={{0,1},{1,2},{2,3},{3,0},{4,5},{5,6},{6,7},{7,4},{8,9},{9,10},{10,1... | collective-permute-start | bytes 3538952 | tf_op jit(solution)/shard_map/ppermute | solution.py:17
  72.5 26.4 %collective-permute-start.3 = (bf16[8,36,2048]{2,0,1:T(8,128)(2,1)S(1)}, bf16[8,36,2048]{2,0,1:T(8,128)(2,1)}, u32[]{:S(2)}, u32[]{:S(2)}) collective-permute-start(bf16[8,36,2048]{2,0,1:T(8,128)(2,1)S(1)} %collective-permute-done.2), channel_id=1, source_target_pairs={{0,1},{1,2},{2,3},{3,0},{4,5},{5,6},{6,7},{7,4},{8,9},{9,10},{10,1... | collective-permute-start | bytes 3538952 | tf_op jit(solution)/shard_map/ppermute | solution.py:17
  72.5 29.1 %collective-permute-start.4 = (bf16[8,36,2048]{2,0,1:T(8,128)(2,1)}, bf16[8,36,2048]{2,0,1:T(8,128)(2,1)S(1)}, u32[]{:S(2)}, u32[]{:S(2)}) collective-permute-start(bf16[8,36,2048]{2,0,1:T(8,128)(2,1)} %copy-done.4), channel_id=1, source_target_pairs={{0,3},{1,0},{2,1},{3,2},{4,7},{5,4},{6,5},{7,6},{8,11},{9,8},{10,9... | collective-permute-start | bytes 3538952 | tf_op jit(solution)/shard_map/ppermute | solution.py:19
  101.5 8.5 %slice-start = ((s8[7340032]{0:T(1024)(128)(4,1)}), s8[4194304]{0:T(1024)(128)(4,1)S(1)}, s32[]{:S(2)}) async-start(s8[7340032]{0:T(1024)(128)(4,1)} %bitcast.138), calls=%async_computation.6 | async-start | bytes 8388608
  102.3 7.8 %slice-start.1 = ((s8[7340032]{0:T(1024)(128)(4,1)}), s8[3145728]{0:T(1024)(128)(4,1)S(1)}, s32[]{:S(2)}) async-start(s8[7340032]{0:T(1024)(128)(4,1)} %bitcast.138), calls=%async_computation.7 | async-start | bytes 6291456
  106.0 4.0 %copy-start.2 = (bf16[64,36,2048]{2,1,0:T(8,128)(2,1)}, bf16[64,36,2048]{2,1,0:T(8,128)(2,1)S(1)}, u32[]{:S(2)}) copy-start(bf16[64,36,2048]{2,1,0:T(8,128)(2,1)S(1)} %copy_dynamic-update-slice_fusion.1) | copy-start | bytes 28311556
  122.1 30.9 %copy-start.5 = (bf16[1024,64]{0,1:T(8,128)(2,1)S(1)}, bf16[1024,64]{0,1:T(8,128)(2,1)}, u32[]{:S(2)}) copy-start(bf16[1024,64]{0,1:T(8,128)(2,1)} %param.15) | copy-start | bytes 393220
  122.1 30.9 %copy-start.6 = (bf16[1024,64]{0,1:T(8,128)(2,1)S(1)}, bf16[1024,64]{0,1:T(8,128)(2,1)}, u32[]{:S(2)}) copy-start(bf16[1024,64]{0,1:T(8,128)(2,1)} %param.16) | copy-start | bytes 393220
  152.9 9.5 %copy-start.3 = (bf16[1024,256]{1,0:T(8,128)(2,1)S(1)}, bf16[1024,256]{1,0:T(8,128)(2,1)}, u32[]{:S(2)}) copy-start(bf16[1024,256]{1,0:T(8,128)(2,1)} %param.14) | copy-start | bytes 1572868
  152.9 9.5 %copy-start.7 = (f32[4]{0:T(128)S(1)}, f32[4]{0:T(128)}, u32[]{:S(2)}) copy-start(f32[4]{0:T(128)} %param.17) | copy-start | bytes 52
  152.9 99.2 %reduce-scatter.3.cloned.1.call-start = ((), (), s32[]{:S(2)}) async-start(), calls=%async_computation.4 | async-start | bytes 5242880 | tf_op jit(solution)/shard_map/reduce_scatter | solution.py:109
  153.0 5.0 %collective-permute-start = (bf16[128,128]{0,1:T(8,128)(2,1)S(1)}, bf16[128,128]{0,1:T(8,128)(2,1)S(1)}, u32[]{:S(2)}, u32[]{:S(2)}) collective-permute-start(bf16[128,128]{0,1:T(8,128)(2,1)S(1)} %get-tuple-element.131), channel_id=1, source_target_pairs={{0,4},{4,8},{8,12},{12,16},{16,20},{20,24},{24,28},{1,5},{5,9},{9,... | collective-permute-start | bytes 98312 | tf_op jit(solution)/shard_map/ppermute | solution.py:31
  156.5 5.8 %collective-permute-start.1 = (bf16[128,128]{0,1:T(8,128)(2,1)S(1)}, bf16[128,128]{0,1:T(8,128)(2,1)S(1)}, u32[]{:S(2)}, u32[]{:S(2)}) collective-permute-start(bf16[128,128]{0,1:T(8,128)(2,1)S(1)} %get-tuple-element.132), channel_id=1, source_target_pairs={{4,0},{8,4},{12,8},{16,12},{20,16},{24,20},{28,24},{5,1},{9,5},{13... | collective-permute-start | bytes 98312 | tf_op jit(solution)/shard_map/ppermute | solution.py:32
  166.2 2.7 %copy-start.1 = (f32[768,512,4]{1,0,2:T(8,128)}, f32[768,512,4]{1,0,2:T(8,128)S(1)}, u32[]{:S(2)}) copy-start(f32[768,512,4]{1,0,2:T(8,128)S(1)} %get-tuple-element.182) | copy-start | bytes 18874372 | tf_op jit(solution)/shard_map/while
  179.1 2.7 %copy-start.1 = (f32[768,512,4]{1,0,2:T(8,128)}, f32[768,512,4]{1,0,2:T(8,128)S(1)}, u32[]{:S(2)}) copy-start(f32[768,512,4]{1,0,2:T(8,128)S(1)} %get-tuple-element.182) | copy-start | bytes 18874372 | tf_op jit(solution)/shard_map/while
  187.9 22.0 %copy-start.8 = (f32[128,2]{0,1:T(2,128)S(1)}, f32[128,2]{0,1:T(2,128)}, u32[]{:S(2)}) copy-start(f32[128,2]{0,1:T(2,128)} %param.22) | copy-start | bytes 3076
  204.4 36.8 %all-to-all-start.1 = ((bf16[8,36,2048]{2,1,0:T(8,128)(2,1)}), bf16[8,36,2048]{2,1,0:T(8,128)(2,1)}, u32[]{:S(2)}, u32[]{:S(2)}) async-start(bf16[8,36,2048]{2,1,0:T(8,128)(2,1)} %reduce-scatter.5.cloned.1.call-done), calls=%async_computation.3 | async-start | bytes 2621440 | tf_op jit(solution)/shard_map/all_to_all | solution.py:150
Sparse Core Ops, SparseCore 0:
  153.0 51.2 reduce-scatter.4
  207.5 44.5 reduce-scatter.2
